TPU v7x, 512 devices: a whole 4x8x8 slice. The times are simulated.
512 devices in a mesh: ep: 32 (over z, x), tp: 16 (over y, core).
Axes of the slice: x: 4, y: 8, z: 8, core: 2. Of those that a mesh axis runs over, the one named last changes fastest.
Arguments:
- mix_query: bfloat16 [8192, 2048], P('ep', 'tp'), may hold values from -6 to 6
- forget_input: bfloat16 [8192, 2048], P('ep', 'tp'), may hold values from -6 to 6
- mix_value: bfloat16 [8192, 2048], P('ep', 'tp'), may hold values from -6 to 6
- out_gate_input: bfloat16 [8192, 2048], P('ep', 'tp'), may hold values from -6 to 6
- decay_shift: float32 [8192, 16], P('ep', 'tp'), may hold values from -1.5 to 0
- forget_floor: float32 [2048], P('tp'), may hold values from 0.9 to 1
- head_gain: float32 [128], replicated, may hold values from 0.1 to 1.9
- w_mix_out: bfloat16 [2048, 2048], P(None, 'tp'), may hold values from -0.125 to 0.125
- moe_input: bfloat16 [8192, 2048], P('ep'), may hold values from -6 to 6
- moe_gain: float32 [2048], replicated, may hold values from 0.1 to 1.9
- routes: int32 [8192, 2], P('ep'), may hold values from 0 to 31, all different within a row; in each aligned block of 256 rows (0 to 255, 256 to 511, ...) at most 20 rows name the same one
- route_weight: float32 [8192, 2], P('ep'), may hold values from 0.1 to 1
- w_exp_gate: bfloat16 [32, 2048, 4096], P('ep', None, 'tp'), may hold values from -0.125 to 0.125
- w_exp_up: bfloat16 [32, 2048, 4096], P('ep', None, 'tp'), may hold values from -0.125 to 0.125
- w_exp_down: bfloat16 [32, 4096, 2048], P('ep', 'tp'), may hold values from -0.125 to 0.125
Outputs:
- mixed: bfloat16 [8192, 2048], P('ep', 'tp')
- moe_out: bfloat16 [8192, 2048], P('ep', 'tp')
Inputs may be any that keep to these rules, and one draw needn't show every extreme that they name: `routes`: at most 20 of the rows of one index of ep name one expert, and in every draw some device's rows name one expert exactly 20 times; the experts of a row differ.
All inputs are finite; a program needn't handle non-finite values.
Results may differ from a plain program's by a relative error of at most 0.02.
Values may be sent and summed in bfloat16 or wider, within the bound.
A program may use at most 64 MiB of HBM per device.

v0:
```python
import jax
import jax.numpy as jnp
from jax import lax
from jax.sharding import Mesh
from jax.sharding import PartitionSpec as P

TOP_K = 2
EP = ("ep_0", "ep_1")
TP = ("tp_0", "tp_1")
eps = 1e-06
highest_precision = lax.Precision.HIGHEST


def nothing_yet(shard, identity):
    return jax.tree.map(
        lambda a, e: jnp.broadcast_to(jnp.asarray(e, a.dtype), a.shape), shard, identity
    )


def gathered_once(shard, axis):
    leaves = jax.tree.leaves(shard)
    sequence = sorted(range(len(leaves)), key=lambda k: -leaves[k].size)
    width = (1, *leaves[sequence[0]].shape)[-1]
    lines = [
        jnp.pad(leaves[k].reshape(-1), (0, -leaves[k].size % width)).reshape(-1, width)
        for k in sequence
    ]
    both, at, found = (lax.all_gather(jnp.concatenate(lines), axis), 0, {})
    for k, line in zip(sequence, lines):
        slab = both[:, at : at + len(line)].reshape(len(both), -1)
        found[k] = slab[:, : leaves[k].size].reshape(-1, *leaves[k].shape)
        at += len(line)
    numbers = iter(range(len(leaves)))
    return jax.tree.map(lambda _: found[next(numbers)], shard)


def carried_in(shard, axes, combine, identity):
    before = start = nothing_yet(shard, identity)
    running = shard
    for axis in reversed(axes):
        peers, index = (lax.axis_size(axis), lax.axis_index(axis))
        pieces = gathered_once(
            jax.tree.map(
                lambda part, kind: part.astype(kind), running, (jnp.bfloat16, jnp.bfloat16)
            ),
            axis,
        )
        inside, running = (start, start)
        for k in range(peers):
            passed = k < index
            running = combine(
                running, jax.tree.map(lambda part, own: part[k].astype(own.dtype), pieces, shard)
            )
            inside = jax.tree.map(lambda new, old: jnp.where(passed, new, old), running, inside)
        before = combine(inside, before)
    return before


def sent_to_all(shard, axis):
    peers = lax.axis_size(axis)
    return lax.all_to_all(
        jnp.broadcast_to(shard[None], (peers, *shard.shape)), axis, 0, 0, tiled=True
    )


def laid_out(tiles, dim):
    tiles = jnp.moveaxis(tiles, 0, dim)
    lengths = tiles.shape
    return tiles.reshape(*lengths[:dim], lengths[dim] * lengths[dim + 1], *lengths[dim + 2 :])


def gather_directly(shard, axis, dim):
    tiles = sent_to_all(shard, axis)
    return laid_out(tiles, dim)


def split_up(shard, dim, peers):
    lengths = shard.shape
    tiles = shard.reshape(*lengths[:dim], peers, lengths[dim] // peers, *lengths[dim + 1 :])
    return jnp.moveaxis(tiles, dim, 0)


def scatter_pairs(shard, chips, core, dim):
    sizes = (lax.axis_size(chips), lax.axis_size(core))
    tiles = split_up(shard, dim, sizes[0] * sizes[1])
    inside = tiles.shape[1:]
    tiles = tiles.reshape(*sizes, *inside).swapaxes(0, 1).reshape(-1, *inside)
    tiles = lax.psum_scatter(tiles, core, scatter_dimension=0, tiled=True)
    return lax.psum_scatter(tiles, chips, scatter_dimension=0, tiled=True)[0]


def chain_step(earlier, later):
    return (earlier[0] * later[0], later[0][:, :, None] * earlier[1] + later[1])


def token_mixer(
    mix_query,
    forget_input,
    mix_value,
    out_gate_input,
    decay_shift,
    forget_floor,
    head_gain,
    w_mix_out,
):
    length = mix_query.shape[0]
    heads_here = decay_shift.shape[1]
    head_size = head_gain.shape[0]
    gate_input = forget_input.astype(jnp.float32)
    forget = forget_floor + (1.0 - forget_floor) * jax.nn.sigmoid(gate_input)
    input_gate = (1.0 - forget_floor) * jax.nn.sigmoid(-gate_input)
    log_decay = jnp.log(forget) + jnp.repeat(decay_shift, head_size, axis=1)

    def by_head(array):
        return array.reshape(length, heads_here, head_size).transpose(1, 0, 2)

    running_decay = jnp.cumsum(by_head(log_decay), axis=1)
    query_rows = by_head(mix_query.astype(jnp.float32)) * jnp.exp(running_decay)
    head_keys = by_head(input_gate)
    values = by_head(mix_value.astype(jnp.float32))
    scores = jnp.einsum(
        "htk,hsk->hts", query_rows, head_keys * jnp.exp(-running_decay), precision=highest_precision
    )
    causal = jnp.arange(length)[:, None] >= jnp.arange(length)[None, :]
    scores = jnp.where(causal[None, :, :], scores, 0.0)
    within_block_output = jnp.einsum("hts,hsv->htv", scores, values, precision=highest_precision)
    closing_total = running_decay[:, -1, :]
    carried_over_state = jnp.einsum(
        "gbx,gbi->gxi",
        head_keys * jnp.exp(closing_total[:, None, :] - running_decay),
        values,
        precision=highest_precision,
    )
    incoming_state = carried_in(
        (jnp.exp(closing_total), carried_over_state),
        EP,
        chain_step,
        (jnp.ones_like(closing_total), jnp.zeros_like(carried_over_state)),
    )[1]
    block_result = within_block_output + jnp.einsum(
        "rsd,rda->rsa", query_rows, incoming_state, precision=highest_precision
    )
    inverse = lax.rsqrt(jnp.mean(block_result * block_result, axis=2, keepdims=True) + eps)
    gated = by_head(jax.nn.silu(out_gate_input.astype(jnp.float32)))
    normed_heads = (block_result * inverse * head_gain * gated).transpose(1, 0, 2)
    head_out = normed_heads.reshape(length, heads_here * head_size).astype(jnp.bfloat16)
    mixed = jnp.dot(
        lax.all_gather(head_out, TP, axis=1, tiled=True),
        w_mix_out,
        preferred_element_type=jnp.float32,
    )
    return mixed.astype(jnp.bfloat16)


def experts_layer(moe_input, moe_gain, routes, route_weight, w_exp_gate, w_exp_up, w_exp_down):
    row_count = moe_input.shape[0]
    expert_count = lax.axis_size(EP)
    capacity = 5 * row_count * TOP_K // (4 * expert_count)
    token_rows = moe_input.astype(jnp.float32)
    inverse = lax.rsqrt(jnp.mean(token_rows * token_rows, axis=1, keepdims=True) + eps)
    normed = (token_rows * inverse * moe_gain).astype(jnp.bfloat16)
    flat_ids = routes.reshape(-1)
    pair_count = flat_ids.shape[0]
    one_hot = (flat_ids[:, None] == jnp.arange(expert_count, dtype=jnp.int32)[None, :]).astype(
        jnp.int32
    )
    earlier_count = jnp.cumsum(one_hot, axis=0) - one_hot
    ranks = jnp.sum(earlier_count * one_hot, axis=1)
    slot_ids = flat_ids * capacity + ranks
    owners = (
        jnp.zeros((expert_count * capacity,), jnp.int32)
        .at[slot_ids]
        .set(jnp.arange(pair_count, dtype=jnp.int32) // TOP_K)
    )
    filled = (
        jnp.zeros((expert_count * capacity,), jnp.bfloat16)
        .at[slot_ids]
        .set(jnp.ones((pair_count,), jnp.bfloat16))
    )
    outgoing = normed[owners] * filled[:, None]
    w_gate = w_exp_gate[0]
    w_up = w_exp_up[0]
    w_down = w_exp_down[0]
    width = normed.shape[1] // lax.axis_size(TP)
    own_slice = lax.dynamic_slice_in_dim(outgoing, lax.axis_index(TP) * width, width, 1)
    arrived = lax.all_to_all(own_slice, EP, split_axis=0, concat_axis=0, tiled=True)
    portion = gather_directly(arrived, TP, 1)
    gate_sum = jnp.dot(portion, w_gate, preferred_element_type=jnp.float32)
    up_sum = jnp.dot(portion, w_up, preferred_element_type=jnp.float32)
    hidden = (jax.nn.silu(gate_sum) * up_sum).astype(jnp.bfloat16)
    partial_value = jnp.dot(hidden, w_down, preferred_element_type=jnp.float32)
    summed = (
        scatter_pairs(partial_value.astype(jnp.bfloat16), "tp_0", "tp_1", 1)
        .astype(jnp.float32)
        .astype(jnp.bfloat16)
    )
    returned = lax.all_to_all(summed, EP, split_axis=0, concat_axis=0, tiled=True)
    picked = returned[slot_ids].astype(jnp.float32).reshape(row_count, TOP_K, returned.shape[1])
    combined = jnp.sum(picked * route_weight[:, :, None], axis=1)
    return combined.astype(jnp.bfloat16)


def body(
    mix_query,
    forget_input,
    mix_value,
    out_gate_input,
    decay_shift,
    forget_floor,
    head_gain,
    w_mix_out,
    moe_input,
    moe_gain,
    routes,
    route_weight,
    w_exp_gate,
    w_exp_up,
    w_exp_down,
):
    mixed = token_mixer(
        mix_query,
        forget_input,
        mix_value,
        out_gate_input,
        decay_shift,
        forget_floor,
        head_gain,
        w_mix_out,
    )
    moe_out = experts_layer(
        moe_input, moe_gain, routes, route_weight, w_exp_gate, w_exp_up, w_exp_down
    )
    return (mixed, moe_out)


def solution(mesh):
    torus = Mesh(mesh.devices.reshape(8, 4, 8, 2), ("ep_0", "ep_1", "tp_0", "tp_1"))
    placed = (
        P(EP, TP),
        P(EP, TP),
        P(EP, TP),
        P(EP, TP),
        P(EP, TP),
        P(TP),
        P(),
        P(None, TP),
        P(EP, None),
        P(),
        P(EP, None),
        P(EP, None),
        P(EP, None, TP),
        P(EP, None, TP),
        P(EP, TP, None),
    )
    return jax.shard_map(
        body, mesh=torus, in_specs=placed, out_specs=(P(EP, TP), P(EP, TP)), check_vma=False
    )
```

profile of v0, /device:TPU:1, one launch (start us, length us, event | category | flops | bytes accessed | tf_op | source)
XLA Modules:
  0.0 226.4 jit_solution(9882331451542621476)
XLA Ops:
  8.1 0.9 copy.57
  9.0 0.1 eq.29
  9.2 0.1 eq.25
  9.3 0.7 broadcast_multiply_fusion
  10.0 1.2 reduce-window.16
  11.2 0.2 slice_reduce_fusion
  11.5 0.1 copy.56
  11.6 0.1 mul.373
  11.9 2.4 %scatter_custom_fusion = s32[640]{0:T(1024)S(1)} fusion(s32[512]{0:T(512)S(1)} %bitcast.177, s32[512]{0:T(512)S(1)} %add_select_fusion, s32[]{:T(128)} %constant.34.clone.1), kind=kCustom, calls=%fused_computation.173 | custom fusion | bytes 2564 | tf_op jit(solution)/shard_map/scatter | solution.py:173
  14.3 1.5 fusion
  15.9 1.0 fusion.2
  16.9 4.1 %gather_fusion = bf16[640,2048]{1,0:T(8,128)(2,1)} fusion(bf16[256,2048]{1,0:T(8,128)(2,1)S(1)} %fusion.2, s32[1024]{0:T(1024)S(1)} %pad_clamp_fusion.1), kind=kCustom, calls=%fused_computation | custom fusion | bytes 5245440 | tf_op jit(solution)/shard_map/gather | solution.py:180
  21.0 3.8 %scatter_custom_fusion.1 = bf16[640]{0:T(1024)(128)(2,1)S(1)} fusion(s32[512]{0:T(512)S(1)} %bitcast.178, bf16[512]{0:T(512)(128)(2,1)S(1)} %broadcast.266, bf16[]{:T(256)} %constant.85.clone.1), kind=kCustom, calls=%fused_computation.177 | custom fusion | bytes 1282 | tf_op jit(solution)/shard_map/scatter | solution.py:178
  24.7 1.1 dynamic-slice_multiply_fusion
  25.9 23.5 %all_to_all.26 = bf16[32,20,128]{2,1,0:T(8,128)(2,1)S(1)} all-to-all(bf16[32,20,128]{2,1,0:T(8,128)(2,1)S(1)} %all_to_all.17), channel_id=1, replica_groups=mesh['ep_0'=8,'ep_1'=4,'tp_0'=8,'tp_1'=2] {'ep_0','ep_1'}, dimensions={0} | all-to-all | bytes 327680 | tf_op jit(solution)/shard_map/all_to_all | solution.py:186
  49.4 0.2 copy.60
  49.6 0.3 broadcast_in_dim.28
  49.9 71.8 %all_to_all.27 = bf16[16,640,128]{1,2,0:T(8,128)(2,1)S(1)} all-to-all(bf16[16,640,128]{1,2,0:T(8,128)(2,1)S(1)} %broadcast_in_dim.28), channel_id=1, replica_groups=mesh['ep_0'=8,'ep_1'=4,'tp_0'=8,'tp_1'=2] {'tp_0','tp_1'}, dimensions={0} | all-to-all | bytes 5242880 | tf_op jit(solution)/shard_map/all_to_all | solution.py:61
  121.7 1.5 copy-done.2
  123.2 0.9 fusion.7
  124.1 0.3 copy-done.13
  124.4 6.1 %fusion.3 = bf16[80,16,8,128]{3,2,1,0:T(8,128)(2,1)} fusion(bf16[1,256,2048]{2,1,0:T(8,128)(2,1)S(1)} %copy-done, bf16[640,2048]{0,1:T(8,128)(2,1)} %bitcast.175, bf16[1,2048,256]{2,1,0:T(8,128)(2,1)S(1)} %copy-done.13, f32[640,256]{1,0:T(8,128)S(1)} %fusion.7), kind=kOutput, calls=%fused_computation.11 | convolution fusion | flops 1344471040 | bytes 7995392 | tf_op jit(solution)/shard_map/dot_general | solution.py:191
  130.5 2.4 %copy.68 = bf16[80,16,8,128]{3,2,0,1:T(8,128)(2,1)S(1)} copy(bf16[80,16,8,128]{3,2,1,0:T(8,128)(2,1)} %fusion.3) | data formatting | bytes 5242880 | tf_op jit(solution)/shard_map/reshape | solution.py:79
  132.9 1.7 copy.62
  134.8 0.7 copy-done.5
  135.8 0.1 copy.52
  135.9 0.1 fusion.156
  136.1 0.1 copy.53
  136.3 0.1 copy.54
  136.4 0.2 broadcast.258
  136.8 0.2 slice_reduce_fusion.1
  137.0 0.2 fusion.93
  137.2 0.3 convolution_convert_fusion.2
  137.5 9.5 %all-gather.2 = bf16[4,129,128]{2,1,0:T(8,128)(2,1)S(1)} all-gather(bf16[1,129,128]{2,1,0:T(8,128)(2,1)S(1)} %maximum_bitcast_fusion), channel_id=2, replica_groups=mesh['ep_0'=8,'ep_1'=4,'tp_0'=8,'tp_1'=2] {'ep_1'}, dimensions={0}, use_global_device_ids=true | all-gather | bytes 165120 | tf_op jit(solution)/shard_map/all_gather | solution.py:28
  147.4 0.1 fusion.94
  147.6 19.3 %all-gather.3 = bf16[8,129,128]{2,1,0:T(8,128)(2,1)S(1)} all-gather(bf16[1,129,128]{2,1,0:T(8,128)(2,1)S(1)} %maximum_bitcast_fusion.1), channel_id=3, replica_groups=mesh['ep_0'=8,'ep_1'=4,'tp_0'=8,'tp_1'=2] {'ep_0'}, dimensions={0}, use_global_device_ids=true | all-gather | bytes 297216 | tf_op jit(solution)/shard_map/all_gather | solution.py:28
  166.8 0.4 convolution_select_fusion
  167.3 0.3 fusion.157
  167.6 0.6 multiply_reduce_fusion
  168.2 0.7 fusion.42
  169.0 17.1 %reduce-scatter.5.cloned.1.call-done = bf16[1,640,128]{2,1,0:T(8,128)(2,1)} async-done(((bf16[8,640,128]{2,1,0:T(8,128)(2,1)}), bf16[1,640,128]{2,1,0:T(8,128)(2,1)}) %reduce-scatter.5.cloned.1.call-update) | async-done | bytes 163856 | tf_op jit(solution)/shard_map/reduce_scatter | solution.py:89
  186.1 1.6 all_to_all.20
  187.7 9.9 %all-to-all-start.2 = ((bf16[32,20,128]{2,1,0:T(8,128)(2,1)}), bf16[32,20,128]{2,1,0:T(8,128)(2,1)S(1)}, u32[]{:S(2)}, u32[]{:S(2)}) async-start(bf16[32,20,128]{2,1,0:T(8,128)(2,1)} %all_to_all.20), calls=%async_computation.4 | async-start | bytes 393216 | tf_op jit(solution)/shard_map/all_to_all | solution.py:197
  197.6 0.1 copy.63
  197.8 16.4 %all-gather.6.cloned.1.call-done = bf16[256,2048]{0,1:T(8,128)(2,1)} async-done(((bf16[256,128]{0,1:T(8,128)(2,1)}), bf16[256,2048]{0,1:T(8,128)(2,1)}) %all-gather.6.cloned.1.call-update) | async-done | bytes 1048592 | tf_op jit(solution)/shard_map/all_gather | solution.py:148
  214.1 2.3 %convolution_convert_fusion.1 = bf16[256,128]{1,0:T(8,128)(2,1)} fusion(bf16[256,2048]{0,1:T(8,128)(2,1)} %all-gather.6.cloned.1.call-done, bf16[2048,128]{1,0:T(8,128)(2,1)S(1)} %copy-done.3), kind=kOutput, calls=%fused_computation.16 | convolution fusion | flops 134250496 | bytes 1638400 | tf_op jit(solution)/shard_map/dot_general | solution.py:147
  216.5 1.3 gather_fusion.1
  217.9 1.1 fusion.12
  (67 shorter events, 1.4 us)
Async XLA Ops:
  8.0 116.1 %copy-start = (bf16[1,256,2048]{2,1,0:T(8,128)(2,1)S(1)}, bf16[1,256,2048]{2,1,0:T(8,128)(2,1)}, u32[]{:S(2)}) copy-start(bf16[1,256,2048]{2,1,0:T(8,128)(2,1)} %param.29) | copy-start | bytes 3145732
  8.0 7.9 %copy-start.1 = (bf16[256,2048]{1,0:T(8,128)(2,1)S(1)}, bf16[256,2048]{1,0:T(8,128)(2,1)}, u32[]{:S(2)}) copy-start(bf16[256,2048]{1,0:T(8,128)(2,1)} %param.23) | copy-start | bytes 3145732
  8.0 139.0 %reduce-scatter.3.cloned.1.call-start = ((), (), s32[]{:S(2)}) async-start(), calls=%async_computation.6 | async-start | bytes 3932160 | tf_op jit(solution)/shard_map/reduce_scatter | solution.py:88
  49.9 73.3 %copy-start.12 = (bf16[1,2048,256]{2,1,0:T(8,128)(2,1)S(1)}, bf16[1,2048,256]{2,1,0:T(8,128)(2,1)}, u32[]{:S(2)}) copy-start(bf16[1,2048,256]{2,1,0:T(8,128)(2,1)} %param.27) | copy-start | bytes 3145732
  121.7 1.5 copy-start.2
  123.2 1.2 copy-start.13
  134.6 0.8 copy-start.5
  134.6 1.0 copy-start.10
  134.6 1.0 copy-start.9
  134.7 2.6 %copy-start.4 = (bf16[256,128]{1,0:T(8,128)(2,1)S(1)}, bf16[256,128]{1,0:T(8,128)(2,1)}, u32[]{:S(2)}) copy-start(bf16[256,128]{1,0:T(8,128)(2,1)} %param.17) | copy-start | bytes 196612
  134.7 12.4 %copy-start.6 = (bf16[256,128]{1,0:T(8,128)(2,1)S(1)}, bf16[256,128]{1,0:T(8,128)(2,1)}, u32[]{:S(2)}) copy-start(bf16[256,128]{1,0:T(8,128)(2,1)} %param.15) | copy-start | bytes 196612
  134.7 12.6 %copy-start.7 = (bf16[256,128]{1,0:T(8,128)(2,1)S(1)}, bf16[256,128]{1,0:T(8,128)(2,1)}, u32[]{:S(2)}) copy-start(bf16[256,128]{1,0:T(8,128)(2,1)} %param.18) | copy-start | bytes 196612
  134.7 51.4 %reduce-scatter.5.cloned.1.call-start = ((), (), s32[]{:S(2)}) async-start(), calls=%async_computation.7 | async-start | bytes 1474560 | tf_op jit(solution)/shard_map/reduce_scatter | solution.py:89
  137.5 30.8 %copy-start.11 = (f32[128]{0:T(128)S(1)}, f32[128]{0:T(128)}, u32[]{:S(2)}) copy-start(f32[128]{0:T(128)} %param.21) | copy-start | bytes 1540
  147.0 50.6 %copy-start.8 = (f32[256,2]{0,1:T(2,128)S(1)}, f32[256,2]{0,1:T(2,128)}, u32[]{:S(2)}) copy-start(f32[256,2]{0,1:T(2,128)} %param.26) | copy-start | bytes 6148
  147.0 67.1 %copy-start.3 = (bf16[2048,128]{1,0:T(8,128)(2,1)S(1)}, bf16[2048,128]{1,0:T(8,128)(2,1)}, u32[]{:S(2)}) copy-start(bf16[2048,128]{1,0:T(8,128)(2,1)} %param.22) | copy-start | bytes 1572868
  147.0 67.1 %all-gather.6.cloned.1.call-start = ((), (), s32[]{:S(2)}) async-start(), calls=%async_computation.5 | async-start | bytes 1114112 | tf_op jit(solution)/shard_map/all_gather | solution.py:148
  187.7 28.8 %all-to-all-start.2 = ((bf16[32,20,128]{2,1,0:T(8,128)(2,1)}), bf16[32,20,128]{2,1,0:T(8,128)(2,1)S(1)}, u32[]{:S(2)}, u32[]{:S(2)}) async-start(bf16[32,20,128]{2,1,0:T(8,128)(2,1)} %all_to_all.20), calls=%async_computation.4 | async-start | bytes 393216 | tf_op jit(solution)/shard_map/all_to_all | solution.py:197
Sparse Core Ops, SparseCore 0:
  134.8 9.7 reduce-scatter.2
  147.4 38.5 reduce-scatter.4
Sparse Core Ops, SparseCore 1:
  169.1 45.0 all-gather.5
where the time goes:
time: 227 us; the launch traced here: 226 us
  blocking collectives  124 us (55%)
  waiting for transfers between devices  33.5 us (15%)
  local copies, waits for them, and re-layouts  23.8 us (10%)
  between operations  16 us (7%)
  matrix products  11 us (5%)
  starting transfers between devices  10 us (4%)
  other arithmetic  8.08 us (4%)
    all_to_all x1, blocking collectives, sent_to_all(): lax.all_to_all(jnp.broadcast_to(shard[None], (peers, *shard.shape)), axis...  71.8 us
    all_gather x2, blocking collectives, gathered_once(): both, at, found = (lax.all_gather(jnp.concatenate(lines), axis), 0, {})  28.7 us
    all_to_all x1, blocking collectives, experts_layer(): lax.all_to_all(own_slice, EP, split_axis=0, concat_axis=0, tiled=True)  23.5 us
    reduce_scatter x1, waiting for transfers between devices, scatter_pairs(): return lax.psum_scatter(tiles, chips, scatter_dimension=0, tiled=True)[0]  17.1 us
    all_gather x1, waiting for transfers between devices, token_mixer(): lax.all_gather(head_out, TP, axis=1, tiled=True)  16.4 us
    all_to_all x1, starting transfers between devices, experts_layer(): lax.all_to_all(summed, EP, split_axis=0, concat_axis=0, tiled=True)  9.92 us
    dot_general x1, matrix products, experts_layer(): partial_value = jnp.dot(hidden, w_down, preferred_element_type=jnp.float32)  6.11 us
  transfers between devices with their start and end apart: 4, of which 2 were waited for; matrix products, arithmetic and copies ran while one was open for 3% of the time, Pallas kernels for 0%

commit v1 on v0

--- a/solution.py
+++ b/solution.py
@@ -9,6 +9,13 @@
 TP = ("tp_0", "tp_1")
 eps = 1e-06
 highest_precision = lax.Precision.HIGHEST
+
+
+def swapped_in(value, axis, d):
+    count = lax.axis_size(axis)
+    blocks = jnp.stack([value for _ in range(count)])
+    blocks = lax.all_to_all(blocks, axis, split_axis=0, concat_axis=0)
+    return jnp.concatenate(blocks, axis=d)
 
 
 def nothing_yet(shard, identity):
@@ -144,11 +151,7 @@
     gated = by_head(jax.nn.silu(out_gate_input.astype(jnp.float32)))
     normed_heads = (block_result * inverse * head_gain * gated).transpose(1, 0, 2)
     head_out = normed_heads.reshape(length, heads_here * head_size).astype(jnp.bfloat16)
-    mixed = jnp.dot(
-        lax.all_gather(head_out, TP, axis=1, tiled=True),
-        w_mix_out,
-        preferred_element_type=jnp.float32,
-    )
+    mixed = jnp.dot(swapped_in(head_out, TP, 1), w_mix_out, preferred_element_type=jnp.float32)
     return mixed.astype(jnp.bfloat16)
 
 

time: 227 us -> 251 us (1.11); the launches traced: 226 us -> 248 us
  waiting for transfers between devices: 33.5 us -> 50.3 us
  starting transfers between devices: 10 us -> 17.4 us
    reduce_scatter x1, waiting for transfers between devices: 17.1 us -> 41.5 us  [scatter_pairs(): return lax.psum_scatter(tiles, chips, scatter_dimension=0, tiled=True)[0]]
    all_gather x1 -> x0, waiting for transfers between devices: 16.4 us -> none  [token_mixer(): lax.all_gather(head_out, TP, axis=1, tiled=True)]
    all_to_all x0 -> x1, starting transfers between devices: none -> 11.7 us  [swapped_in(): blocks = lax.all_to_all(blocks, axis, split_axis=0, concat_axis=0)]
    all_to_all x1, waiting for transfers between devices: 0.01 us -> 8.68 us  [experts_layer(): lax.all_to_all(summed, EP, split_axis=0, concat_axis=0, tiled=True)]
    all_to_all x1, starting transfers between devices: 9.92 us -> 5.61 us  [experts_layer(): lax.all_to_all(summed, EP, split_axis=0, concat_axis=0, tiled=True)]
  transfers between devices with their start and end apart: 4 -> 4, of which waited for: 2 -> 2; matrix products, arithmetic and copies ran while one was open for 3% -> 2% of each run, Pallas kernels for 0% -> 0%
where the time goes in v1:
time: 251 us; the launch traced here: 248 us
  blocking collectives  124 us (49%)
  waiting for transfers between devices  50.3 us (20%)
  local copies, waits for them, and re-layouts  24.9 us (10%)
  starting transfers between devices  17.4 us (7%)
  between operations  14.6 us (6%)
  matrix products  9.74 us (4%)
  other arithmetic  7.45 us (3%)
    all_to_all x1, blocking collectives, sent_to_all(): lax.all_to_all(jnp.broadcast_to(shard[None], (peers, *shard.shape)), axis...  71.8 us
    reduce_scatter x1, waiting for transfers between devices, scatter_pairs(): return lax.psum_scatter(tiles, chips, scatter_dimension=0, tiled=True)[0]  41.5 us
    all_gather x2, blocking collectives, gathered_once(): both, at, found = (lax.all_gather(jnp.concatenate(lines), axis), 0, {})  28.2 us
    all_to_all x1, blocking collectives, experts_layer(): lax.all_to_all(own_slice, EP, split_axis=0, concat_axis=0, tiled=True)  23.5 us
    all_to_all x1, starting transfers between devices, swapped_in(): blocks = lax.all_to_all(blocks, axis, split_axis=0, concat_axis=0)  11.7 us
    all_to_all x1, waiting for transfers between devices, experts_layer(): lax.all_to_all(summed, EP, split_axis=0, concat_axis=0, tiled=True)  8.68 us
    dot_general x1, matrix products, experts_layer(): partial_value = jnp.dot(hidden, w_down, preferred_element_type=jnp.float32)  6.11 us
    all_to_all x1, starting transfers between devices, experts_layer(): lax.all_to_all(summed, EP, split_axis=0, concat_axis=0, tiled=True)  5.61 us
  transfers between devices with their start and end apart: 4, of which 2 were waited for; matrix products, arithmetic and copies ran while one was open for 2% of the time, Pallas kernels for 0%

profile of v1, /device:TPU:1, one launch (start us, length us, event | category | flops | bytes accessed | tf_op | source)
XLA Modules:
  0.0 247.8 jit_solution(2324633150962991951)
XLA Ops:
  7.2 0.9 copy.58
  8.2 0.1 eq.29
  8.3 0.1 eq.25
  8.5 0.7 broadcast_multiply_fusion
  9.2 1.2 reduce-window.16
  10.4 0.2 slice_reduce_fusion
  10.6 0.1 copy.57
  10.8 0.1 mul.373
  11.0 2.4 scatter_custom_fusion
  13.5 1.5 fusion
  15.0 1.0 fusion.2
  16.0 4.1 %gather_fusion = bf16[640,2048]{1,0:T(8,128)(2,1)} fusion(bf16[256,2048]{1,0:T(8,128)(2,1)S(1)} %fusion.2, s32[1024]{0:T(1024)S(1)} %pad_clamp_fusion.1), kind=kCustom, calls=%fused_computation | custom fusion | bytes 5245440 | tf_op jit(solution)/shard_map/gather | solution.py:183
  20.1 3.8 %scatter_custom_fusion.1 = bf16[640]{0:T(1024)(128)(2,1)S(1)} fusion(s32[512]{0:T(512)S(1)} %bitcast.182, bf16[512]{0:T(512)(128)(2,1)S(1)} %broadcast.267, bf16[]{:T(256)} %constant.85.clone.1), kind=kCustom, calls=%fused_computation.177 | custom fusion | bytes 1282 | tf_op jit(solution)/shard_map/scatter | solution.py:181
  23.9 1.1 dynamic-slice_multiply_fusion
  25.0 23.5 %all_to_all.31 = bf16[32,20,128]{2,1,0:T(8,128)(2,1)S(1)} all-to-all(bf16[32,20,128]{2,1,0:T(8,128)(2,1)S(1)} %all_to_all.21), channel_id=1, replica_groups=mesh['ep_0'=8,'ep_1'=4,'tp_0'=8,'tp_1'=2] {'ep_0','ep_1'}, dimensions={0} | all-to-all | bytes 327680 | tf_op jit(solution)/shard_map/all_to_all | solution.py:189
  48.6 0.2 copy.61
  48.7 0.3 broadcast_in_dim.28
  49.0 71.8 %all_to_all.32 = bf16[16,640,128]{1,2,0:T(8,128)(2,1)S(1)} all-to-all(bf16[16,640,128]{1,2,0:T(8,128)(2,1)S(1)} %broadcast_in_dim.28), channel_id=1, replica_groups=mesh['ep_0'=8,'ep_1'=4,'tp_0'=8,'tp_1'=2] {'tp_0','tp_1'}, dimensions={0} | all-to-all | bytes 5242880 | tf_op jit(solution)/shard_map/all_to_all | solution.py:68
  120.8 1.5 copy-done.2
  122.4 0.9 fusion.7
  123.2 0.3 copy-done.13
  123.6 6.1 %fusion.3 = bf16[80,16,8,128]{3,2,1,0:T(8,128)(2,1)} fusion(bf16[1,256,2048]{2,1,0:T(8,128)(2,1)S(1)} %copy-done, bf16[640,2048]{0,1:T(8,128)(2,1)} %bitcast.179, bf16[1,2048,256]{2,1,0:T(8,128)(2,1)S(1)} %copy-done.13, f32[640,256]{1,0:T(8,128)S(1)} %fusion.7), kind=kOutput, calls=%fused_computation.11 | convolution fusion | flops 1344471040 | bytes 7995392 | tf_op jit(solution)/shard_map/dot_general | solution.py:194
  129.7 2.4 copy.69
  132.1 1.7 copy.63
  133.9 0.7 copy-done.5
  135.1 0.1 fusion.156
  135.2 0.1 copy.54
  135.4 0.1 copy.55
  135.5 0.2 broadcast.259
  136.3 0.2 slice_reduce_fusion.1
  136.4 0.2 fusion.93
  136.6 0.3 convolution_convert_fusion.2
  136.9 9.5 %all-gather.2 = bf16[4,129,128]{2,1,0:T(8,128)(2,1)S(1)} all-gather(bf16[1,129,128]{2,1,0:T(8,128)(2,1)S(1)} %maximum_bitcast_fusion), channel_id=2, replica_groups=mesh['ep_0'=8,'ep_1'=4,'tp_0'=8,'tp_1'=2] {'ep_1'}, dimensions={0}, use_global_device_ids=true | all-gather | bytes 165120 | tf_op jit(solution)/shard_map/all_gather | solution.py:35
  146.4 0.1 fusion.94
  146.6 18.8 %all-gather.3 = bf16[8,129,128]{2,1,0:T(8,128)(2,1)S(1)} all-gather(bf16[1,129,128]{2,1,0:T(8,128)(2,1)S(1)} %maximum_bitcast_fusion.1), channel_id=3, replica_groups=mesh['ep_0'=8,'ep_1'=4,'tp_0'=8,'tp_1'=2] {'ep_0'}, dimensions={0}, use_global_device_ids=true | all-gather | bytes 297216 | tf_op jit(solution)/shard_map/all_gather | solution.py:35
  165.4 0.4 convolution_select_fusion
  165.8 0.3 fusion.157
  166.2 0.6 multiply_reduce_fusion
  167.0 1.1 stack.2
  168.1 11.7 %all-to-all-start = ((bf16[16,256,128]{1,2,0:T(8,128)(2,1)}), bf16[16,256,128]{1,2,0:T(8,128)(2,1)S(1)}, u32[]{:S(2)}, u32[]{:S(2)}) async-start(bf16[16,256,128]{1,2,0:T(8,128)(2,1)} %stack.2), calls=%async_computation | async-start | bytes 2097152 | tf_op jit(solution)/shard_map/all_to_all | solution.py:17
  179.8 41.5 %reduce-scatter.5.cloned.1.call-done = bf16[1,640,128]{2,1,0:T(8,128)(2,1)} async-done(((bf16[8,640,128]{2,1,0:T(8,128)(2,1)}), bf16[1,640,128]{2,1,0:T(8,128)(2,1)}) %reduce-scatter.5.cloned.1.call-update) | async-done | bytes 163856 | tf_op jit(solution)/shard_map/reduce_scatter | solution.py:96
  221.3 1.6 all_to_all.24
  222.9 5.6 %all-to-all-start.3 = ((bf16[32,20,128]{2,1,0:T(8,128)(2,1)}), bf16[32,20,128]{2,1,0:T(8,128)(2,1)S(1)}, u32[]{:S(2)}, u32[]{:S(2)}) async-start(bf16[32,20,128]{2,1,0:T(8,128)(2,1)} %all_to_all.24), calls=%async_computation.5 | async-start | bytes 393216 | tf_op jit(solution)/shard_map/all_to_all | solution.py:200
  228.6 0.1 copy.64
  228.7 1.1 convolution_convert_fusion.1
  229.8 8.7 %all-to-all-done.3 = bf16[32,20,128]{2,1,0:T(8,128)(2,1)S(1)} async-done(((bf16[32,20,128]{2,1,0:T(8,128)(2,1)}), bf16[32,20,128]{2,1,0:T(8,128)(2,1)S(1)}, u32[]{:S(2)}, u32[]{:S(2)}) %all-to-all-start.3) | async-done | bytes 163872 | tf_op jit(solution)/shard_map/all_to_all | solution.py:200
  238.6 1.3 gather_fusion.1
  239.9 1.1 fusion.12
  (67 shorter events, 1.5 us)
Async XLA Ops:
  7.2 116.1 %copy-start = (bf16[1,256,2048]{2,1,0:T(8,128)(2,1)S(1)}, bf16[1,256,2048]{2,1,0:T(8,128)(2,1)}, u32[]{:S(2)}) copy-start(bf16[1,256,2048]{2,1,0:T(8,128)(2,1)} %param.29) | copy-start | bytes 3145732
  7.2 7.9 %copy-start.1 = (bf16[256,2048]{1,0:T(8,128)(2,1)S(1)}, bf16[256,2048]{1,0:T(8,128)(2,1)}, u32[]{:S(2)}) copy-start(bf16[256,2048]{1,0:T(8,128)(2,1)} %param.23) | copy-start | bytes 3145732
  7.2 159.0 %reduce-scatter.3.cloned.1.call-start = ((), (), s32[]{:S(2)}) async-start(), calls=%async_computation.6 | async-start | bytes 3932160 | tf_op jit(solution)/shard_map/reduce_scatter | solution.py:95
  49.0 73.3 %copy-start.12 = (bf16[1,2048,256]{2,1,0:T(8,128)(2,1)S(1)}, bf16[1,2048,256]{2,1,0:T(8,128)(2,1)}, u32[]{:S(2)}) copy-start(bf16[1,2048,256]{2,1,0:T(8,128)(2,1)} %param.27) | copy-start | bytes 3145732
  120.8 1.5 copy-start.2
  122.4 1.2 copy-start.13
  133.8 0.8 copy-start.5
  133.8 1.0 copy-start.10
  133.8 1.0 copy-start.9
  133.8 2.2 copy-start.6
  133.8 2.3 copy-start.7
  133.8 2.8 %copy-start.4 = (bf16[256,128]{1,0:T(8,128)(2,1)S(1)}, bf16[256,128]{1,0:T(8,128)(2,1)}, u32[]{:S(2)}) copy-start(bf16[256,128]{1,0:T(8,128)(2,1)} %param.17) | copy-start | bytes 196612
  133.9 87.4 %reduce-scatter.5.cloned.1.call-start = ((), (), s32[]{:S(2)}) async-start(), calls=%async_computation.7 | async-start | bytes 1474560 | tf_op jit(solution)/shard_map/reduce_scatter | solution.py:96
  136.9 29.9 %copy-start.11 = (f32[128]{0:T(128)S(1)}, f32[128]{0:T(128)}, u32[]{:S(2)}) copy-start(f32[128]{0:T(128)} %param.21) | copy-start | bytes 1540
  166.2 62.4 %copy-start.8 = (f32[256,2]{0,1:T(2,128)S(1)}, f32[256,2]{0,1:T(2,128)}, u32[]{:S(2)}) copy-start(f32[256,2]{0,1:T(2,128)} %param.26) | copy-start | bytes 6148
  166.2 62.5 %copy-start.3 = (bf16[2048,128]{1,0:T(8,128)(2,1)S(1)}, bf16[2048,128]{1,0:T(8,128)(2,1)}, u32[]{:S(2)}) copy-start(bf16[2048,128]{1,0:T(8,128)(2,1)} %param.22) | copy-start | bytes 1572868
  168.1 54.9 %all-to-all-start = ((bf16[16,256,128]{1,2,0:T(8,128)(2,1)}), bf16[16,256,128]{1,2,0:T(8,128)(2,1)S(1)}, u32[]{:S(2)}, u32[]{:S(2)}) async-start(bf16[16,256,128]{1,2,0:T(8,128)(2,1)} %stack.2), calls=%async_computation | async-start | bytes 2097152 | tf_op jit(solution)/shard_map/all_to_all | solution.py:17
  222.9 15.6 %all-to-all-start.3 = ((bf16[32,20,128]{2,1,0:T(8,128)(2,1)}), bf16[32,20,128]{2,1,0:T(8,128)(2,1)S(1)}, u32[]{:S(2)}, u32[]{:S(2)}) async-start(bf16[32,20,128]{2,1,0:T(8,128)(2,1)} %all_to_all.24), calls=%async_computation.5 | async-start | bytes 393216 | tf_op jit(solution)/shard_map/all_to_all | solution.py:200
Sparse Core Ops, SparseCore 0:
  134.0 9.7 reduce-scatter.2
  166.3 54.9 reduce-scatter.4
